TPU v7x, 32 devices: a whole 2x2x4 slice. The times are simulated.
32 devices in a mesh: sp: 4 (over z), fs: 4 (over y, x), tp: 2 (over core).
Axes of the slice: x: 2, y: 2, z: 4, core: 2. Of those that a mesh axis runs over, the one named last changes fastest.
Arguments:
- tokens: bfloat16 [4, 1536, 2048], P('fs', ('sp', 'tp')), may hold values from -6 to 6
- norm_gain: float32 [2048], replicated, may hold values from 0.1 to 1.9
- conv_gate_w: bfloat16 [2048, 1024], P('sp', 'tp'), may hold values from -0.125 to 0.125
- conv_in_w: bfloat16 [2048, 1024], P('sp', 'tp'), may hold values from -0.125 to 0.125
- query_w: bfloat16 [2048, 1024], P('sp', 'tp'), may hold values from -0.125 to 0.125
- forget_w: bfloat16 [2048, 1024], P('sp', 'tp'), may hold values from -0.125 to 0.125
- value_w: bfloat16 [2048, 1024], P('sp', 'tp'), may hold values from -0.125 to 0.125
- conv_taps: float32 [3, 1024], P(None, 'tp'), may hold values from -3.5 to 3.5
- floor_gate: float32 [1024], P('tp'), may hold values from 0.93 to 1
- leak: float32 [4, 1536, 8], P('fs', 'sp', 'tp'), may hold values from -1.4 to 0
- head_gain: float32 [128], replicated, may hold values from 0.1 to 1.9
- conv_out_w: bfloat16 [1024, 2048], P('tp', 'fs'), may hold values from -0.125 to 0.125
- chain_out_w: bfloat16 [1024, 2048], P('tp', 'fs'), may hold values from -0.125 to 0.125
Outputs:
- mixed: bfloat16 [4, 1536, 2048], P('fs', ('sp', 'tp'))
All inputs are finite; a program needn't handle non-finite values.
Results may differ from a plain program's by a relative error of at most 0.013.
Values may be sent and summed in bfloat16 or wider, within the bound.
A program may use at most 128 MiB of HBM per device.

v0:
```python
import jax
import jax.numpy as jnp
from jax import lax
from jax.sharding import PartitionSpec as P

BLOCK = 64
HIGH_ACCURACY = lax.Precision.HIGHEST


def as_sent(array):

    def short(part):
        return part.astype(jnp.bfloat16) if part.dtype == jnp.float32 else part

    return jax.tree.map(short, array)


def passed_along(array, axis, by):
    count = lax.axis_size(axis)
    pairs = [(i, i + by) for i in range(count) if 0 <= i + by < count]
    return lax.ppermute(array, axis, pairs)


def entering(value, axis, join, neutral):
    count, mine = (lax.axis_size(axis), lax.axis_index(axis))
    pieces = jax.tree.map(lambda part: lax.all_gather(part, axis), value)
    subtotal = jax.tree.map(
        lambda part, zero: jnp.full_like(part, 0) + jnp.asarray(zero, part.dtype), value, neutral
    )

    def hop(position, subtotal):
        longer = join(subtotal, jax.tree.map(lambda part: part[position], pieces))
        return jax.tree.map(lambda new, old: jnp.where(position < mine, new, old), longer, subtotal)

    return lax.fori_loop(0, count - 1, hop, subtotal)


def norm_rows(matrix, norm_gain):
    values = matrix.astype(jnp.float32)
    center = values - jnp.mean(values, axis=-1, keepdims=True)
    spread = jnp.mean(center * center, axis=-1, keepdims=True)
    return (center * lax.rsqrt(spread + 1e-05) * norm_gain).astype(jnp.bfloat16)


def block_chain(query, keys, values, decay):
    heads, length, width = query.shape
    count = length // BLOCK

    def split_blocks(array):
        return array.reshape(heads, count, BLOCK, array.shape[-1]).transpose(1, 0, 2, 3)

    causal = jnp.tril(jnp.ones((BLOCK, BLOCK), jnp.float32))

    def advance(hidden_state, inputs):
        query_part, key_portion, value_portion, decay_part = inputs
        running_state = jnp.cumsum(decay_part, axis=1)
        scaled_query = query_part * jnp.exp(running_state)
        key_scaled = key_portion * jnp.exp(-running_state)
        scores = (
            jnp.einsum("htk,hsk->hts", scaled_query, key_scaled, precision=HIGH_ACCURACY) * causal
        )
        inside = jnp.einsum("hts,hsv->htv", scores, value_portion, precision=HIGH_ACCURACY)
        carried_state = jnp.einsum(
            "rgn,rns->rgs", scaled_query, hidden_state, precision=HIGH_ACCURACY
        )
        final_state = running_state[:, -1:, :]
        state_update = jnp.einsum(
            "qdm,qdt->qmt",
            key_portion * jnp.exp(final_state - running_state),
            value_portion,
            precision=HIGH_ACCURACY,
        )
        return (
            jnp.exp(final_state[:, 0, :])[:, :, None] * hidden_state + state_update,
            inside + carried_state,
        )

    initial = jnp.zeros((heads, width, values.shape[-1]), jnp.float32)
    hidden_state, layer_results = lax.scan(
        advance,
        initial,
        (split_blocks(query), split_blocks(keys), split_blocks(values), split_blocks(decay)),
    )
    return (
        layer_results.transpose(1, 0, 2, 3).reshape(heads, length, values.shape[-1]),
        hidden_state,
    )


def chain_join(earlier_tokens, later):
    return (
        earlier_tokens[0] + later[0],
        jnp.exp(later[0])[:, :, None] * earlier_tokens[1] + later[1],
    )


def body(
    tokens,
    norm_gain,
    conv_gate_w,
    conv_in_w,
    query_w,
    forget_w,
    value_w,
    conv_taps,
    floor_gate,
    leak,
    head_gain,
    conv_out_w,
    chain_out_w,
):
    own_rows = norm_rows(tokens[0], norm_gain)
    normed = lax.all_gather(own_rows, "tp", axis=0, tiled=True)
    length = normed.shape[0]
    weights = (conv_gate_w, conv_in_w, query_w, forget_w, value_w)
    groups = lax.axis_size("fs")
    member = lax.axis_index("fs")
    sliced = tuple(
        (
            lax.dynamic_slice_in_dim(
                weight, member * (weight.shape[1] // groups), weight.shape[1] // groups, 1
            )
            for weight in weights
        )
    )
    pooled = lax.all_gather(normed[None], "fs", axis=0, tiled=True)
    flat_rows = pooled.reshape(groups * length, pooled.shape[2])
    pieces = jax.tree.map(
        lambda part: lax.all_gather(part, "sp", axis=0, tiled=True), as_sent(sliced)
    )
    sums = tuple(
        (jnp.dot(flat_rows, piece, preferred_element_type=jnp.float32) for piece in pieces)
    )
    quarters = tuple(
        (total.astype(jnp.bfloat16).reshape(groups, length, total.shape[1]) for total in sums)
    )
    returned = jax.tree.map(
        lambda part, own: part.astype(own.dtype),
        lax.all_to_all(as_sent(quarters), "fs", split_axis=0, concat_axis=2, tiled=True),
        quarters,
    )
    projected = tuple((column_set[0] for column_set in returned))
    second_gate, signal, query_raw, forget_raw, value_raw = projected
    margin = conv_taps.shape[0] - 1
    rim = passed_along(signal[length - margin :], "sp", 1)
    padded = jnp.concatenate([rim, signal], axis=0).astype(jnp.float32)
    filtered = jnp.zeros((length, signal.shape[1]), jnp.float32)
    for offset in range(margin + 1):
        filtered = filtered + conv_taps[offset] * padded[offset : offset + length]
    conv_mix = (second_gate.astype(jnp.float32) * filtered).astype(jnp.bfloat16)
    heads_here = leak.shape[2]
    head_width = query_raw.shape[1] // heads_here

    def by_head(array):
        return array.astype(jnp.float32).reshape(length, heads_here, head_width).transpose(1, 0, 2)

    floor = floor_gate.reshape(heads_here, 1, head_width)
    logits = by_head(forget_raw)
    retain = floor + (1.0 - floor) * jax.nn.sigmoid(logits)
    keys = (1.0 - floor) * jax.nn.sigmoid(-logits)
    decay = jnp.log(retain) + leak[0].T[:, :, None]
    query = jax.nn.silu(by_head(query_raw))
    pairwise_dot, hidden_state = block_chain(query, keys, by_head(value_raw), decay)
    total_decay = jnp.sum(decay, axis=1)
    identity = (jnp.zeros_like(total_decay), jnp.zeros_like(hidden_state))
    earlier_tokens = entering((total_decay, hidden_state), "sp", chain_join, identity)
    filter_reach = query * jnp.exp(jnp.cumsum(decay, axis=1))
    recurrence_raw = pairwise_dot + jnp.einsum(
        "rgn,rns->rgs", filter_reach, earlier_tokens[1], precision=HIGH_ACCURACY
    )
    scale = lax.rsqrt(jnp.mean(recurrence_raw * recurrence_raw, axis=-1, keepdims=True) + 1e-06)
    chain_mix = (
        (recurrence_raw * scale * head_gain)
        .transpose(1, 0, 2)
        .reshape(length, heads_here * head_width)
        .astype(jnp.bfloat16)
    )
    conv_full, chain_full = (
        lax.all_gather(conv_out_w, "fs", axis=1, tiled=True),
        lax.all_gather(chain_out_w, "fs", axis=1, tiled=True),
    )
    mixed = lax.psum_scatter(
        jnp.dot(conv_mix, conv_full, preferred_element_type=jnp.float32)
        + jnp.dot(chain_mix, chain_full, preferred_element_type=jnp.float32),
        "tp",
        scatter_dimension=0,
        tiled=True,
    )
    return mixed.astype(jnp.bfloat16)[None]


def solution(mesh):
    in_specs = (
        P("fs", ("sp", "tp"), None),
        P(),
        P("sp", "tp"),
        P("sp", "tp"),
        P("sp", "tp"),
        P("sp", "tp"),
        P("sp", "tp"),
        P(None, "tp"),
        P("tp"),
        P("fs", "sp", "tp"),
        P(),
        P("tp", "fs"),
        P("tp", "fs"),
    )
    out_specs = P("fs", ("sp", "tp"), None)
    return jax.shard_map(body, mesh=mesh, in_specs=in_specs, out_specs=out_specs, check_vma=False)
```

profile of v0, /device:TPU:0, one launch (start us, length us, event | category | flops | bytes accessed | tf_op | source)
XLA Modules:
  0.0 289.1 jit_solution(1176081124464315372)
XLA Ops:
  6.5 1.4 convert_reduce_fusion
  8.0 1.5 fusion.29
  9.5 2.0 fusion.31
  11.6 12.6 %all-gather.10.cloned.1.call-done = bf16[384,2048]{1,0:T(8,128)(2,1)} async-done(((bf16[192,2048]{1,0:T(8,128)(2,1)}), bf16[384,2048]{1,0:T(8,128)(2,1)}) %all-gather.10.cloned.1.call-update) | async-done | bytes 1572880 | tf_op jit(solution)/shard_map/all_gather | solution.py:113
  24.3 0.7 all-gather.12.cloned.1.call-update
  25.0 16.3 %all_gather.44 = bf16[2048,128]{1,0:T(8,128)(2,1)S(1)} all-gather(bf16[512,128]{1,0:T(8,128)(2,1)S(1)} %constant_dynamic-slice_fusion.2), channel_id=1, replica_groups=mesh['sp'=4,'fs'=4,'tp'=2] {'sp'}, dimensions={0}, use_global_device_ids=true | all-gather | bytes 655360 | tf_op jit(solution)/shard_map/all_gather | solution.py:129
  41.4 0.9 constant_dynamic-slice_fusion
  42.3 16.1 %all_gather.46 = bf16[2048,128]{1,0:T(8,128)(2,1)S(1)} all-gather(bf16[512,128]{1,0:T(8,128)(2,1)S(1)} %constant_dynamic-slice_fusion), channel_id=1, replica_groups=mesh['sp'=4,'fs'=4,'tp'=2] {'sp'}, dimensions={0}, use_global_device_ids=true | all-gather | bytes 655360 | tf_op jit(solution)/shard_map/all_gather | solution.py:129
  58.4 0.9 constant_dynamic-slice_fusion.1
  59.3 15.8 %all_gather.45 = bf16[2048,128]{1,0:T(8,128)(2,1)S(1)} all-gather(bf16[512,128]{1,0:T(8,128)(2,1)S(1)} %constant_dynamic-slice_fusion.1), channel_id=1, replica_groups=mesh['sp'=4,'fs'=4,'tp'=2] {'sp'}, dimensions={0}, use_global_device_ids=true | all-gather | bytes 655360 | tf_op jit(solution)/shard_map/all_gather | solution.py:129
  75.1 22.2 %all-gather.16.cloned.1.call-done = bf16[1536,2048]{1,0:T(8,128)(2,1)} async-done(((bf16[384,2048]{1,0:T(8,128)(2,1)}), bf16[1536,2048]{1,0:T(8,128)(2,1)}) %all-gather.16.cloned.1.call-update) | async-done | bytes 6291472 | tf_op jit(solution)/shard_map/all_gather | solution.py:126
  97.3 5.4 %convolution_convert_fusion.2 = bf16[1536,128]{1,0:T(8,128)(2,1)} fusion(bf16[1536,2048]{1,0:T(8,128)(2,1)} %all-gather.16.cloned.1.call-done, bf16[2048,128]{1,0:T(8,128)(2,1)S(1)} %all_gather.44), kind=kOutput, calls=%fused_computation.38 | convolution fusion | flops 805502976 | bytes 7208960 | tf_op jit(solution)/shard_map/dot_general | solution.py:132
  102.6 3.5 %all-to-all-start.2 = ((bf16[4,384,128]{2,1,0:T(8,128)(2,1)}), bf16[4,384,128]{2,1,0:T(8,128)(2,1)S(1)}, u32[]{:S(2)}, u32[]{:S(2)}) async-start(bf16[4,384,128]{2,1,0:T(8,128)(2,1)} %bitcast.15), calls=%async_computation.2 | async-start | bytes 786432 | tf_op jit(solution)/shard_map/all_to_all | solution.py:139
  106.1 5.7 %convolution_convert_fusion = bf16[1536,128]{1,0:T(8,128)(2,1)} fusion(bf16[1536,2048]{1,0:T(8,128)(2,1)} %all-gather.16.cloned.1.call-done, bf16[2048,128]{1,0:T(8,128)(2,1)S(1)} %all_gather.46), kind=kOutput, calls=%fused_computation.36 | convolution fusion | flops 805502976 | bytes 7208960 | tf_op jit(solution)/shard_map/dot_general | solution.py:132
  111.8 2.6 convolution_convert_fusion.1
  114.4 2.7 all-to-all-done.2
  117.1 3.5 %all-to-all-start.3 = ((bf16[4,384,128]{2,1,0:T(8,128)(2,1)}), bf16[4,384,128]{2,1,0:T(8,128)(2,1)S(1)}, u32[]{:S(2)}, u32[]{:S(2)}) async-start(bf16[4,384,128]{2,1,0:T(8,128)(2,1)} %bitcast.30), calls=%async_computation.3 | async-start | bytes 786432 | tf_op jit(solution)/shard_map/all_to_all | solution.py:139
  121.7 0.8 copy-done.3
  122.5 2.6 add_exponential_fusion
  125.0 2.2 all-to-all-done.3
  127.2 3.5 %all-to-all-start.4 = ((bf16[4,384,128]{2,1,0:T(8,128)(2,1)}), bf16[4,384,128]{2,1,0:T(8,128)(2,1)S(1)}, u32[]{:S(2)}, u32[]{:S(2)}) async-start(bf16[4,384,128]{2,1,0:T(8,128)(2,1)} %bitcast.33), calls=%async_computation.4 | async-start | bytes 786432 | tf_op jit(solution)/shard_map/all_to_all | solution.py:139
  130.8 2.2 copy.35
  133.0 1.9 fusion.52
  134.8 6.2 %all-to-all-done.4 = bf16[4,384,128]{2,1,0:T(8,128)(2,1)S(1)} async-done(((bf16[4,384,128]{2,1,0:T(8,128)(2,1)}), bf16[4,384,128]{2,1,0:T(8,128)(2,1)S(1)}, u32[]{:S(2)}, u32[]{:S(2)}) %all-to-all-start.4) | async-done | bytes 393248 | tf_op jit(solution)/shard_map/all_to_all | solution.py:139
  141.1 2.2 bitcast_multiply_fusion.7
  143.3 20.6 %while.27 = (s32[]{:T(128)}, f32[4,128,128]{2,1,0:T(8,128)S(1)}, f32[6,4,64,128]{3,2,0,1:T(8,128)}, f32[6,4,64,128]{3,2,0,1:T(8,128)}, f32[6,4,64,128]{3,2,0,1:T...) while((s32[]{:T(128)}, f32[4,128,128]{2,1,0:T(8,128)S(1)}, ...), condition=%wide.region_4.5_spmd.clone, body=%wide.region_2.4_spmd.clone.sunk | while | flops 153575424 | bytes 3275900 | solution.py:79
  143.3 0.9 dynamic-slice_bitcast_fusion.2
  145.0 1.0 fusion.86
  146.7 0.9 dynamic-slice_bitcast_fusion.2
  148.4 1.0 fusion.86
  150.2 0.9 dynamic-slice_bitcast_fusion.2
  151.9 1.0 fusion.86
  153.6 0.9 dynamic-slice_bitcast_fusion.2
  155.3 1.0 fusion.86
  157.0 0.9 dynamic-slice_bitcast_fusion.2
  158.7 1.0 fusion.86
  160.5 0.9 dynamic-slice_bitcast_fusion.2
  162.2 1.0 fusion.86
  163.2 0.7 convolution_add_fusion.5
  163.9 0.7 copy-done.1
  164.6 0.9 constant_dynamic-slice_fusion.3
  165.6 0.9 constant_dynamic-slice_fusion.4
  166.5 21.4 %all_gather.42 = bf16[2048,128]{1,0:T(8,128)(2,1)S(1)} all-gather(bf16[512,128]{1,0:T(8,128)(2,1)S(1)} %constant_dynamic-slice_fusion.3), channel_id=1, replica_groups=mesh['sp'=4,'fs'=4,'tp'=2] {'sp'}, dimensions={0}, use_global_device_ids=true | all-gather | bytes 655360 | tf_op jit(solution)/shard_map/all_gather | solution.py:129
  187.9 18.9 %all_gather.41 = bf16[2048,128]{1,0:T(8,128)(2,1)S(1)} all-gather(bf16[512,128]{1,0:T(8,128)(2,1)S(1)} %constant_dynamic-slice_fusion.4), channel_id=1, replica_groups=mesh['sp'=4,'fs'=4,'tp'=2] {'sp'}, dimensions={0}, use_global_device_ids=true | all-gather | bytes 655360 | tf_op jit(solution)/shard_map/all_gather | solution.py:129
  206.9 4.6 %convolution_convert_fusion.3 = bf16[1536,128]{1,0:T(8,128)(2,1)S(1)} fusion(bf16[1536,2048]{1,0:T(8,128)(2,1)} %all-gather.16.cloned.1.call-done, bf16[2048,128]{1,0:T(8,128)(2,1)S(1)} %all_gather.42), kind=kOutput, calls=%fused_computation.39 | convolution fusion | flops 805502976 | bytes 7208960 | tf_op jit(solution)/shard_map/dot_general | solution.py:132
  211.4 1.0 copy.28
  212.4 3.5 %all-to-all-start.1 = ((bf16[4,384,128]{1,2,0:T(8,128)(2,1)}), bf16[4,384,128]{1,2,0:T(8,128)(2,1)S(1)}, u32[]{:S(2)}, u32[]{:S(2)}) async-start(bf16[4,384,128]{1,2,0:T(8,128)(2,1)} %copy.28), calls=%async_computation.1 | async-start | bytes 786432 | tf_op jit(solution)/shard_map/all_to_all | solution.py:139
  215.9 4.6 %convolution_convert_fusion.4 = bf16[1536,128]{1,0:T(8,128)(2,1)S(1)} fusion(bf16[1536,2048]{1,0:T(8,128)(2,1)} %all-gather.16.cloned.1.call-done, bf16[2048,128]{1,0:T(8,128)(2,1)S(1)} %all_gather.41), kind=kOutput, calls=%fused_computation.40 | convolution fusion | flops 805502976 | bytes 7208960 | tf_op jit(solution)/shard_map/dot_general | solution.py:132
  220.5 0.9 copy.27
  221.7 3.9 %all-to-all-start = ((bf16[4,384,128]{1,2,0:T(8,128)(2,1)}), bf16[4,384,128]{1,2,0:T(8,128)(2,1)S(1)}, u32[]{:S(2)}, u32[]{:S(2)}) async-start(bf16[4,384,128]{1,2,0:T(8,128)(2,1)} %copy.27), calls=%async_computation | async-start | bytes 786432 | tf_op jit(solution)/shard_map/all_to_all | solution.py:139
  226.6 2.2 collective-permute-start
  228.9 2.6 all-to-all-done
  231.5 11.9 %all-gather.3 = f32[4,4,128]{2,1,0:T(4,128)S(1)} all-gather(f32[1,4,128]{2,1,0:T(4,128)S(1)} %bitcast.201), channel_id=3, replica_groups=mesh['sp'=4,'fs'=4,'tp'=2] {'sp'}, dimensions={0}, use_global_device_ids=true | all-gather | bytes 10240 | tf_op jit(solution)/shard_map/all_gather | solution.py:26
  243.8 0.7 fusion.50
  244.5 4.2 %fusion.54 = f32[384,2048]{1,0:T(8,128)} fusion(bf16[384,512]{0,1:T(8,128)(2,1)S(1)} %fusion.50, bf16[512,2048]{1,0:T(8,128)(2,1)} %all-gather.12.cloned.1.call-done), kind=kOutput, calls=%fused_computation.99 | convolution fusion | flops 805306368 | bytes 5636096 | tf_op jit(solution)/shard_map/dot_general | solution.py:183
  248.8 3.7 %while.28 = (s32[]{:T(128)}, f32[4,128,128]{2,1,0:T(8,128)S(1)}, s32[]{:T(128)}, f32[4,4,128]{2,1,0:T(4,128)S(1)}, f32[4,4,128,128]{3,2,1,0:T(8,128)}, /*index=5*/s32[]{:T(128)}, s32[]{:T(128)}) while((s32[]{:T(128)}, f32[4,128,128]{2,1,0:T(8,128)S(1)}, s32[]{:T(128)}, f32[4,4,128]{2,1,0:T(4,128)S(1)}, ...), condition=%wide.region_9.10_spmd.clone, body=%wide.region_8.9_spmd.clone.sunk | while | flops 262148 | bytes 792681 | solution.py:35
  248.8 1.2 fusion.87
  250.1 1.2 fusion.87
  251.3 1.2 fusion.87
  252.5 1.1 multiply_reduce_fusion
  253.8 9.6 %all-gather.14.cloned.1.call-done = bf16[512,2048]{1,0:T(8,128)(2,1)} async-done(((bf16[512,512]{1,0:T(8,128)(2,1)}), bf16[512,2048]{1,0:T(8,128)(2,1)}) %all-gather.14.cloned.1.call-update) | async-done | bytes 2097168 | tf_op jit(solution)/shard_map/all_gather | solution.py:180
  263.3 5.2 %convolution_add_fusion.2 = f32[384,2048]{1,0:T(8,128)} fusion(f32[384,2048]{1,0:T(8,128)} %fusion.54, bf16[384,512]{0,1:T(8,128)(2,1)S(1)} %bitcast.187, bf16[512,2048]{1,0:T(8,128)(2,1)} %all-gather.14.cloned.1.call-done), kind=kOutput, calls=%fused_computation.35 | convolution fusion | flops 806092800 | bytes 8781824 | tf_op jit(solution)/shard_map/dot_general | solution.py:184
  268.5 11.3 %reduce-scatter.2.cloned.1.call-done = f32[192,2048]{1,0:T(8,128)} async-done(((f32[384,2048]{1,0:T(8,128)}), f32[192,2048]{1,0:T(8,128)}) %reduce-scatter.2.cloned.1.call-update) | async-done | bytes 1572880 | tf_op jit(solution)/shard_map/reduce_scatter | solution.py:182
  279.9 2.4 convert_bitcast_fusion.2
  (101 shorter events, 11.2 us)
Async XLA Ops:
  6.5 18.4 %copy-start = (bf16[512,512]{1,0:T(8,128)(2,1)S(1)}, bf16[512,512]{1,0:T(8,128)(2,1)}, u32[]{:S(2)}) copy-start(bf16[512,512]{1,0:T(8,128)(2,1)} %param.22) | copy-start | bytes 1572868
  6.5 2.9 %copy-start.2 = (bf16[1,192,2048]{2,1,0:T(8,128)(2,1)S(1)}, bf16[1,192,2048]{2,1,0:T(8,128)(2,1)}, u32[]{:S(2)}) copy-start(bf16[1,192,2048]{2,1,0:T(8,128)(2,1)} %param.17) | copy-start | bytes 2359300
  6.5 17.7 %all-gather.10.cloned.1.call-start = ((), (), s32[]{:S(2)}) async-start(), calls=%async_computation.6 | async-start | bytes 2359296 | tf_op jit(solution)/shard_map/all_gather | solution.py:113
  11.5 29.9 %copy-start.7 = (f32[512]{0:T(512)S(1)}, f32[512]{0:T(512)}, u32[]{:S(2)}) copy-start(f32[512]{0:T(512)} %param.25) | copy-start | bytes 6148
  11.5 85.8 %all-gather.16.cloned.1.call-start = ((), (), s32[]{:S(2)}) async-start(), calls=%async_computation.10 | async-start | bytes 7864320 | tf_op jit(solution)/shard_map/all_gather | solution.py:126
  24.2 220.3 %all-gather.12.cloned.1.call-start = ((), (), s32[]{:S(2)}) async-start(), calls=%async_computation.7 | async-start | bytes 2621440 | tf_op jit(solution)/shard_map/all_gather | solution.py:179
  102.6 14.4 %all-to-all-start.2 = ((bf16[4,384,128]{2,1,0:T(8,128)(2,1)}), bf16[4,384,128]{2,1,0:T(8,128)(2,1)S(1)}, u32[]{:S(2)}, u32[]{:S(2)}) async-start(bf16[4,384,128]{2,1,0:T(8,128)(2,1)} %bitcast.15), calls=%async_computation.2 | async-start | bytes 786432 | tf_op jit(solution)/shard_map/all_to_all | solution.py:139
  106.1 5.7 %copy-start.11 = (bf16[1536,2048]{1,0:T(8,128)(2,1)S(1)}, bf16[1536,2048]{1,0:T(8,128)(2,1)}, u32[]{:S(2)}) copy-start(bf16[1536,2048]{1,0:T(8,128)(2,1)} %all-gather.16.cloned.1.call-done) | copy-start | bytes 18874372
  111.8 8.7 %copy-start.6 = (f32[1,384,4]{1,2,0:T(4,128)S(1)}, f32[1,384,4]{1,2,0:T(4,128)}, u32[]{:S(2)}) copy-start(f32[1,384,4]{1,2,0:T(4,128)} %param.26) | copy-start | bytes 18436
  117.1 10.1 %all-to-all-start.3 = ((bf16[4,384,128]{2,1,0:T(8,128)(2,1)}), bf16[4,384,128]{2,1,0:T(8,128)(2,1)S(1)}, u32[]{:S(2)}, u32[]{:S(2)}) async-start(bf16[4,384,128]{2,1,0:T(8,128)(2,1)} %bitcast.30), calls=%async_computation.3 | async-start | bytes 786432 | tf_op jit(solution)/shard_map/all_to_all | solution.py:139
  121.4 1.0 copy-start.3
  127.2 13.9 %all-to-all-start.4 = ((bf16[4,384,128]{2,1,0:T(8,128)(2,1)}), bf16[4,384,128]{2,1,0:T(8,128)(2,1)S(1)}, u32[]{:S(2)}, u32[]{:S(2)}) async-start(bf16[4,384,128]{2,1,0:T(8,128)(2,1)} %bitcast.33), calls=%async_computation.4 | async-start | bytes 786432 | tf_op jit(solution)/shard_map/all_to_all | solution.py:139
  130.7 118.1 %all-gather.18.cloned.1.call-start = ((), (), s32[]{:S(2)}) async-start(), calls=%async_computation.11 | async-start | bytes 1310720 | tf_op jit(solution)/shard_map/all_gather | solution.py:26
  163.9 0.7 copy-start.1
  212.4 9.3 %all-to-all-start.1 = ((bf16[4,384,128]{1,2,0:T(8,128)(2,1)}), bf16[4,384,128]{1,2,0:T(8,128)(2,1)S(1)}, u32[]{:S(2)}, u32[]{:S(2)}) async-start(bf16[4,384,128]{1,2,0:T(8,128)(2,1)} %copy.28), calls=%async_computation.1 | async-start | bytes 786432 | tf_op jit(solution)/shard_map/all_to_all | solution.py:139
  220.4 5.8 %copy-start.9 = (f32[3,512]{1,0:T(4,128)S(1)}, f32[3,512]{1,0:T(4,128)}, u32[]{:S(2)}) copy-start(f32[3,512]{1,0:T(4,128)} %param.24) | copy-start | bytes 18436
  220.5 5.8 %copy-start.5 = (f32[6,4,64,128]{3,2,0,1:T(8,128)S(1)}, f32[6,4,64,128]{3,2,0,1:T(8,128)}, u32[]{:S(2)}) copy-start(f32[6,4,64,128]{3,2,0,1:T(8,128)} %get-tuple-element.142) | copy-start | bytes 2359300
  221.4 10.1 %copy-start.8 = (f32[4,128]{1,0:T(4,128)S(1)}, f32[4,128]{1,0:T(4,128)}, u32[]{:S(2)}) copy-start(f32[4,128]{1,0:T(4,128)} %get-tuple-element.227) | copy-start | bytes 6148
  221.7 9.7 %all-to-all-start = ((bf16[4,384,128]{1,2,0:T(8,128)(2,1)}), bf16[4,384,128]{1,2,0:T(8,128)(2,1)S(1)}, u32[]{:S(2)}, u32[]{:S(2)}) async-start(bf16[4,384,128]{1,2,0:T(8,128)(2,1)} %copy.27), calls=%async_computation | async-start | bytes 786432 | tf_op jit(solution)/shard_map/all_to_all | solution.py:139
  225.6 37.8 %all-gather.14.cloned.1.call-start = ((), (), s32[]{:S(2)}) async-start(), calls=%async_computation.8 | async-start | bytes 2621440 | tf_op jit(solution)/shard_map/all_gather | solution.py:180
  226.1 53.7 %reduce-scatter.2.cloned.1.call-start = ((), (), s32[]{:S(2)}) async-start(), calls=%async_computation.9 | async-start | bytes 4718592 | tf_op jit(solution)/shard_map/reduce_scatter | solution.py:182
  226.6 16.8 %collective-permute-start = (bf16[2,512]{0,1:T(8,128)(2,1)S(1)}, bf16[2,512]{0,1:T(8,128)(2,1)S(1)}, u32[]{:S(2)}, u32[]{:S(2)}) collective-permute-start(bf16[2,512]{0,1:T(8,128)(2,1)S(1)} %bitcast.195), channel_id=1, source_target_pairs={{0,8},{8,16},{16,24},{1,9},{9,17},{17,25},{2,10},{10,18},{18,26},{... | collective-permute-start | bytes 6152 | tf_op jit(solution)/shard_map/ppermute | solution.py:21
  248.8 3.7 %copy-start.4 = (f32[4,384,128]{2,1,0:T(8,128)S(1)}, f32[4,384,128]{2,1,0:T(8,128)}, u32[]{:S(2)}) copy-start(f32[4,384,128]{2,1,0:T(8,128)} %get-tuple-element.229) | copy-start | bytes 2359300
  252.4 1.2 copy-start.10
Sparse Core Ops, SparseCore 0:
  11.6 12.5 all-gather.9
  26.0 71.1 all-gather.15
  99.1 42.9 all-gather.11
  164.8 37.6 all-gather.17
  227.9 35.3 all-gather.13
  268.6 11.1 reduce-scatter.1
where the time goes:
time: 290 us; the launch traced here: 289 us
  blocking collectives  101 us (35%)
  waiting for transfers between devices  71 us (24%)
  matrix products  47.2 us (16%)
  other arithmetic  20.8 us (7%)
  starting transfers between devices  20.1 us (7%)
  local copies, waits for them, and re-layouts  15.3 us (5%)
  between operations  13.8 us (5%)
    all_gather x5, blocking collectives, body(): lax.all_gather(part, 'sp', axis=0, tiled=True)  88.6 us
    dot_general x5, matrix products, body(): jnp.dot(flat_rows, piece, preferred_element_type=jnp.float32)  22.8 us
    all_gather x1, waiting for transfers between devices, body(): pooled = lax.all_gather(normed[None], 'fs', axis=0, tiled=True)  22.2 us
    all_to_all x5, starting transfers between devices, body(): lax.all_to_all(as_sent(quarters), 'fs', split_axis=0, concat_axis=2, tile...  17.7 us
    all_to_all x5, waiting for transfers between devices, body(): lax.all_to_all(as_sent(quarters), 'fs', split_axis=0, concat_axis=2, tile...  14 us
    all_gather x1, waiting for transfers between devices, body(): normed = lax.all_gather(own_rows, 'tp', axis=0, tiled=True)  12.6 us
    all_gather x1, blocking collectives, entering(): pieces = jax.tree.map(lambda part: lax.all_gather(part, axis), value)  11.9 us
    reduce_scatter x1, waiting for transfers between devices, body(): lax.psum_scatter(jnp.dot(conv_mix, conv_full, preferred_element_type=jnp....  11.3 us
  transfers between devices with their start and end apart: 12, of which 9 were waited for; matrix products, arithmetic and copies ran while one was open for 24% of the time, Pallas kernels for 0%

commit v1 on v0

--- a/solution.py
+++ b/solution.py
@@ -123,7 +123,11 @@
             for weight in weights
         )
     )
-    pooled = lax.all_gather(normed[None], "fs", axis=0, tiled=True)
+    mine_x = normed[None]
+    kept_arr = lax.axis_size("fs")
+    z2 = jnp.stack([mine_x] * kept_arr)
+    x_next = lax.all_to_all(z2, "fs", split_axis=0, concat_axis=0)
+    pooled = jnp.concatenate(x_next, axis=0)
     flat_rows = pooled.reshape(groups * length, pooled.shape[2])
     pieces = jax.tree.map(
         lambda part: lax.all_gather(part, "sp", axis=0, tiled=True), as_sent(sliced)

time: 290 us -> 311 us (1.072)
  waiting for transfers between devices: 71 us -> 77.2 us
  starting transfers between devices: 20.1 us -> 25.2 us
  local copies, waits for them, and re-layouts: 15.3 us -> 20.3 us
    all_to_all x0 -> x1, waiting for transfers between devices: none -> 36.7 us  [body(): x_next = lax.all_to_all(z2, 'fs', split_axis=0, concat_axis=0)]
    all_gather x1 -> x0, waiting for transfers between devices: 22.2 us -> none  [body(): pooled = lax.all_gather(normed[None], 'fs', axis=0, tiled=True)]
    all_to_all x5, waiting for transfers between devices: 14 us -> 6.77 us  [body(): lax.all_to_all(as_sent(quarters), 'fs', split_axis=0, concat_axis=2, tile...]
    all_to_all x0 -> x1, starting transfers between devices: none -> 5.26 us  [body(): x_next = lax.all_to_all(z2, 'fs', split_axis=0, concat_axis=0)]
    another operation x1 -> x2, local copies, waits for them, and re-layouts: 0.01 us -> 4.84 us  [the longest x1 4.83 us: body(): z2 = jnp.stack([mine_x] * kept_arr)]
  transfers between devices with their start and end apart: 12 -> 12, of which waited for: 9 -> 8; matrix products, arithmetic and copies ran while one was open for 24% -> 23% of each run, Pallas kernels for 0% -> 0%
where the time goes in v1:
time: 311 us; the launch traced here: 310 us
  blocking collectives  101 us (32%)
  waiting for transfers between devices  77.2 us (25%)
  matrix products  49.8 us (16%)
  starting transfers between devices  25.2 us (8%)
  other arithmetic  21.1 us (7%)
  local copies, waits for them, and re-layouts  20.3 us (7%)
  between operations  15.3 us (5%)
    all_gather x5, blocking collectives, body(): lax.all_gather(part, 'sp', axis=0, tiled=True)  88.6 us
    all_to_all x1, waiting for transfers between devices, body(): x_next = lax.all_to_all(z2, 'fs', split_axis=0, concat_axis=0)  36.7 us
    dot_general x5, matrix products, body(): jnp.dot(flat_rows, piece, preferred_element_type=jnp.float32)  25.3 us
    all_to_all x5, starting transfers between devices, body(): lax.all_to_all(as_sent(quarters), 'fs', split_axis=0, concat_axis=2, tile...  18.5 us
    all_gather x1, waiting for transfers between devices, body(): normed = lax.all_gather(own_rows, 'tp', axis=0, tiled=True)  12.7 us
    all_gather x1, blocking collectives, entering(): pieces = jax.tree.map(lambda part: lax.all_gather(part, axis), value)  11.9 us
    reduce_scatter x1, waiting for transfers between devices, body(): lax.psum_scatter(jnp.dot(conv_mix, conv_full, preferred_element_type=jnp....  11.3 us
    all_gather x1, waiting for transfers between devices, body(): lax.all_gather(chain_out_w, 'fs', axis=1, tiled=True)  8.58 us
  transfers between devices with their start and end apart: 12, of which 8 were waited for; matrix products, arithmetic and copies ran while one was open for 23% of the time, Pallas kernels for 0%

profile of v1, /device:TPU:0, one launch (start us, length us, event | category | flops | bytes accessed | tf_op | source)
XLA Modules:
  0.0 309.9 jit_solution(3195687829998906094)
XLA Ops:
  7.4 1.4 convert_reduce_fusion
  8.8 1.5 fusion.29
  10.2 2.5 fusion.31
  12.7 12.7 %all-gather.8.cloned.1.call-done = bf16[384,2048]{1,0:T(8,128)(2,1)} async-done(((bf16[192,2048]{1,0:T(8,128)(2,1)}), bf16[384,2048]{1,0:T(8,128)(2,1)}) %all-gather.8.cloned.1.call-update) | async-done | bytes 1572880 | tf_op jit(solution)/shard_map/all_gather | solution.py:113
  25.4 4.8 %stack.3 = bf16[4,1,384,2048]{3,2,1,0:T(8,128)(2,1)} broadcast(bf16[384,2048]{1,0:T(8,128)(2,1)} %all-gather.8.cloned.1.call-done), dimensions={2,3} | broadcast | bytes 7864320 | tf_op jit(solution)/shard_map/stack | solution.py:128
  30.2 5.3 %all-to-all-start = ((bf16[4,1,384,2048]{3,2,1,0:T(8,128)(2,1)}), bf16[4,1,384,2048]{3,2,1,0:T(8,128)(2,1)}, u32[]{:S(2)}, u32[]{:S(2)}) async-start(bf16[4,1,384,2048]{3,2,1,0:T(8,128)(2,1)} %stack.3), calls=%async_computation | async-start | bytes 12582912 | tf_op jit(solution)/shard_map/all_to_all | solution.py:129
  36.2 0.9 constant_dynamic-slice_fusion
  37.1 0.9 constant_dynamic-slice_fusion.1
  38.0 16.3 %all_gather.40 = bf16[2048,128]{1,0:T(8,128)(2,1)S(1)} all-gather(bf16[512,128]{1,0:T(8,128)(2,1)S(1)} %constant_dynamic-slice_fusion.2), channel_id=1, replica_groups=mesh['sp'=4,'fs'=4,'tp'=2] {'sp'}, dimensions={0}, use_global_device_ids=true | all-gather | bytes 655360 | tf_op jit(solution)/shard_map/all_gather | solution.py:133
  54.3 16.1 %all_gather.42 = bf16[2048,128]{1,0:T(8,128)(2,1)S(1)} all-gather(bf16[512,128]{1,0:T(8,128)(2,1)S(1)} %constant_dynamic-slice_fusion), channel_id=1, replica_groups=mesh['sp'=4,'fs'=4,'tp'=2] {'sp'}, dimensions={0}, use_global_device_ids=true | all-gather | bytes 655360 | tf_op jit(solution)/shard_map/all_gather | solution.py:133
  70.3 15.9 %all_gather.41 = bf16[2048,128]{1,0:T(8,128)(2,1)S(1)} all-gather(bf16[512,128]{1,0:T(8,128)(2,1)S(1)} %constant_dynamic-slice_fusion.1), channel_id=1, replica_groups=mesh['sp'=4,'fs'=4,'tp'=2] {'sp'}, dimensions={0}, use_global_device_ids=true | all-gather | bytes 655360 | tf_op jit(solution)/shard_map/all_gather | solution.py:133
  86.2 36.7 %all-to-all-done = bf16[4,1,384,2048]{3,2,1,0:T(8,128)(2,1)} async-done(((bf16[4,1,384,2048]{3,2,1,0:T(8,128)(2,1)}), bf16[4,1,384,2048]{3,2,1,0:T(8,128)(2,1)}, u32[]{:S(2)}, u32[]{:S(2)}) %all-to-all-start) | async-done | bytes 6291488 | tf_op jit(solution)/shard_map/all_to_all | solution.py:129
  122.9 5.3 %convolution_convert_fusion.2 = bf16[1536,128]{1,0:T(8,128)(2,1)} fusion(bf16[1536,2048]{1,0:T(8,128)(2,1)} %bitcast.1, bf16[2048,128]{1,0:T(8,128)(2,1)S(1)} %all_gather.40), kind=kOutput, calls=%fused_computation.38 | convolution fusion | flops 805502976 | bytes 7208960 | tf_op jit(solution)/shard_map/dot_general | solution.py:136
  128.3 3.5 %all-to-all-start.3 = ((bf16[4,384,128]{2,1,0:T(8,128)(2,1)}), bf16[4,384,128]{2,1,0:T(8,128)(2,1)S(1)}, u32[]{:S(2)}, u32[]{:S(2)}) async-start(bf16[4,384,128]{2,1,0:T(8,128)(2,1)} %bitcast.16), calls=%async_computation.3 | async-start | bytes 786432 | tf_op jit(solution)/shard_map/all_to_all | solution.py:143
  131.7 5.4 %convolution_convert_fusion = bf16[1536,128]{1,0:T(8,128)(2,1)} fusion(bf16[1536,2048]{1,0:T(8,128)(2,1)} %bitcast.1, bf16[2048,128]{1,0:T(8,128)(2,1)S(1)} %all_gather.42), kind=kOutput, calls=%fused_computation.36 | convolution fusion | flops 805502976 | bytes 7208960 | tf_op jit(solution)/shard_map/dot_general | solution.py:136
  137.1 5.4 %convolution_convert_fusion.1 = bf16[1536,128]{1,0:T(8,128)(2,1)} fusion(bf16[1536,2048]{1,0:T(8,128)(2,1)} %bitcast.1, bf16[2048,128]{1,0:T(8,128)(2,1)S(1)} %all_gather.41), kind=kOutput, calls=%fused_computation.37 | convolution fusion | flops 805502976 | bytes 7208960 | tf_op jit(solution)/shard_map/dot_general | solution.py:136
  142.5 4.2 %all-to-all-start.4 = ((bf16[4,384,128]{2,1,0:T(8,128)(2,1)}), bf16[4,384,128]{2,1,0:T(8,128)(2,1)S(1)}, u32[]{:S(2)}, u32[]{:S(2)}) async-start(bf16[4,384,128]{2,1,0:T(8,128)(2,1)} %bitcast.31), calls=%async_computation.4 | async-start | bytes 786432 | tf_op jit(solution)/shard_map/all_to_all | solution.py:143
  147.8 0.8 copy-done.2
  148.6 2.5 add_exponential_fusion
  151.1 1.4 all-to-all-done.4
  152.6 3.5 %all-to-all-start.5 = ((bf16[4,384,128]{2,1,0:T(8,128)(2,1)}), bf16[4,384,128]{2,1,0:T(8,128)(2,1)S(1)}, u32[]{:S(2)}, u32[]{:S(2)}) async-start(bf16[4,384,128]{2,1,0:T(8,128)(2,1)} %bitcast.34), calls=%async_computation.5 | async-start | bytes 786432 | tf_op jit(solution)/shard_map/all_to_all | solution.py:143
  156.2 2.2 copy.35
  158.4 1.8 fusion.52
  160.2 1.6 all-to-all-done.5
  161.9 2.3 bitcast_multiply_fusion.7
  164.1 20.6 %while.27 = (s32[]{:T(128)}, f32[4,128,128]{2,1,0:T(8,128)S(1)}, f32[6,4,64,128]{3,2,0,1:T(8,128)}, f32[6,4,64,128]{3,2,0,1:T(8,128)}, f32[6,4,64,128]{3,2,0,1:T...) while((s32[]{:T(128)}, f32[4,128,128]{2,1,0:T(8,128)S(1)}, ...), condition=%wide.region_4.5_spmd.clone, body=%wide.region_2.4_spmd.clone.sunk | while | flops 153575424 | bytes 3275900 | solution.py:79
  164.1 0.9 dynamic-slice_bitcast_fusion.2
  165.8 1.0 fusion.86
  166.9 0.7 convolution_add_fusion.5
  167.6 0.9 dynamic-slice_bitcast_fusion.2
  169.3 1.0 fusion.86
  171.0 0.9 dynamic-slice_bitcast_fusion.2
  172.7 1.0 fusion.86
  174.4 0.9 dynamic-slice_bitcast_fusion.2
  176.1 1.0 fusion.86
  177.9 0.9 dynamic-slice_bitcast_fusion.2
  179.6 1.0 fusion.86
  181.3 0.9 dynamic-slice_bitcast_fusion.2
  183.0 1.0 fusion.86
  184.7 0.7 copy-done.1
  185.5 0.9 constant_dynamic-slice_fusion.3
  186.4 0.9 constant_dynamic-slice_fusion.4
  187.3 19.7 %all_gather.38 = bf16[2048,128]{1,0:T(8,128)(2,1)S(1)} all-gather(bf16[512,128]{1,0:T(8,128)(2,1)S(1)} %constant_dynamic-slice_fusion.3), channel_id=1, replica_groups=mesh['sp'=4,'fs'=4,'tp'=2] {'sp'}, dimensions={0}, use_global_device_ids=true | all-gather | bytes 655360 | tf_op jit(solution)/shard_map/all_gather | solution.py:133
  207.0 20.7 %all_gather.37 = bf16[2048,128]{1,0:T(8,128)(2,1)S(1)} all-gather(bf16[512,128]{1,0:T(8,128)(2,1)S(1)} %constant_dynamic-slice_fusion.4), channel_id=1, replica_groups=mesh['sp'=4,'fs'=4,'tp'=2] {'sp'}, dimensions={0}, use_global_device_ids=true | all-gather | bytes 655360 | tf_op jit(solution)/shard_map/all_gather | solution.py:133
  227.7 4.6 %convolution_convert_fusion.3 = bf16[1536,128]{1,0:T(8,128)(2,1)S(1)} fusion(bf16[1536,2048]{1,0:T(8,128)(2,1)} %bitcast.1, bf16[2048,128]{1,0:T(8,128)(2,1)S(1)} %all_gather.38), kind=kOutput, calls=%fused_computation.39 | convolution fusion | flops 805502976 | bytes 7208960 | tf_op jit(solution)/shard_map/dot_general | solution.py:136
  232.3 1.0 copy.28
  233.3 3.5 %all-to-all-start.2 = ((bf16[4,384,128]{1,2,0:T(8,128)(2,1)}), bf16[4,384,128]{1,2,0:T(8,128)(2,1)S(1)}, u32[]{:S(2)}, u32[]{:S(2)}) async-start(bf16[4,384,128]{1,2,0:T(8,128)(2,1)} %copy.28), calls=%async_computation.2 | async-start | bytes 786432 | tf_op jit(solution)/shard_map/all_to_all | solution.py:143
  236.8 4.7 %convolution_convert_fusion.4 = bf16[1536,128]{1,0:T(8,128)(2,1)S(1)} fusion(bf16[1536,2048]{1,0:T(8,128)(2,1)} %bitcast.1, bf16[2048,128]{1,0:T(8,128)(2,1)S(1)} %all_gather.37), kind=kOutput, calls=%fused_computation.40 | convolution fusion | flops 805502976 | bytes 7208960 | tf_op jit(solution)/shard_map/dot_general | solution.py:136
  241.5 1.0 copy.27
  242.6 3.9 %all-to-all-start.1 = ((bf16[4,384,128]{1,2,0:T(8,128)(2,1)}), bf16[4,384,128]{1,2,0:T(8,128)(2,1)S(1)}, u32[]{:S(2)}, u32[]{:S(2)}) async-start(bf16[4,384,128]{1,2,0:T(8,128)(2,1)} %copy.27), calls=%async_computation.1 | async-start | bytes 786432 | tf_op jit(solution)/shard_map/all_to_all | solution.py:143
  247.6 1.3 collective-permute-start
  249.0 3.5 %all-to-all-done.1 = bf16[4,384,128]{1,2,0:T(8,128)(2,1)S(1)} async-done(((bf16[4,384,128]{1,2,0:T(8,128)(2,1)}), bf16[4,384,128]{1,2,0:T(8,128)(2,1)S(1)}, u32[]{:S(2)}, u32[]{:S(2)}) %all-to-all-start.1) | async-done | bytes 393248 | tf_op jit(solution)/shard_map/all_to_all | solution.py:143
  252.5 11.9 %all-gather.2 = f32[4,4,128]{2,1,0:T(4,128)S(1)} all-gather(f32[1,4,128]{2,1,0:T(4,128)S(1)} %bitcast.202), channel_id=2, replica_groups=mesh['sp'=4,'fs'=4,'tp'=2] {'sp'}, dimensions={0}, use_global_device_ids=true | all-gather | bytes 10240 | tf_op jit(solution)/shard_map/all_gather | solution.py:26
  264.8 0.7 fusion.50
  265.5 4.3 %fusion.54 = f32[384,2048]{1,0:T(8,128)} fusion(bf16[384,512]{0,1:T(8,128)(2,1)S(1)} %fusion.50, bf16[512,2048]{1,0:T(8,128)(2,1)} %all-gather.10.cloned.1.call-done), kind=kOutput, calls=%fused_computation.99 | convolution fusion | flops 805306368 | bytes 5636096 | tf_op jit(solution)/shard_map/dot_general | solution.py:187
  269.8 3.7 %while.28 = (s32[]{:T(128)}, f32[4,128,128]{2,1,0:T(8,128)S(1)}, s32[]{:T(128)}, f32[4,4,128]{2,1,0:T(4,128)S(1)}, f32[4,4,128,128]{3,2,1,0:T(8,128)}, /*index=5*/s32[]{:T(128)}, s32[]{:T(128)}) while((s32[]{:T(128)}, f32[4,128,128]{2,1,0:T(8,128)S(1)}, s32[]{:T(128)}, f32[4,4,128]{2,1,0:T(4,128)S(1)}, ...), condition=%wide.region_9.10_spmd.clone, body=%wide.region_8.9_spmd.clone.sunk | while | flops 262148 | bytes 792681 | solution.py:35
  269.8 1.2 fusion.87
  271.1 1.2 fusion.87
  272.3 1.1 fusion.87
  273.5 1.1 multiply_reduce_fusion
  274.8 8.6 %all-gather.12.cloned.1.call-done = bf16[512,2048]{1,0:T(8,128)(2,1)} async-done(((bf16[512,512]{1,0:T(8,128)(2,1)}), bf16[512,2048]{1,0:T(8,128)(2,1)}) %all-gather.12.cloned.1.call-update) | async-done | bytes 2097168 | tf_op jit(solution)/shard_map/all_gather | solution.py:184
  283.3 5.2 %convolution_add_fusion.2 = f32[384,2048]{1,0:T(8,128)} fusion(f32[384,2048]{1,0:T(8,128)} %fusion.54, bf16[384,512]{0,1:T(8,128)(2,1)S(1)} %bitcast.188, bf16[512,2048]{1,0:T(8,128)(2,1)} %all-gather.12.cloned.1.call-done), kind=kOutput, calls=%fused_computation.35 | convolution fusion | flops 806092800 | bytes 8781824 | tf_op jit(solution)/shard_map/dot_general | solution.py:188
  288.5 11.3 %reduce-scatter.2.cloned.1.call-done = f32[192,2048]{1,0:T(8,128)} async-done(((f32[384,2048]{1,0:T(8,128)}), f32[192,2048]{1,0:T(8,128)}) %reduce-scatter.2.cloned.1.call-update) | async-done | bytes 1572880 | tf_op jit(solution)/shard_map/reduce_scatter | solution.py:186
  299.9 2.4 convert_bitcast_fusion.2
  (97 shorter events, 11.6 us)
Async XLA Ops:
  7.4 28.8 %copy-start = (bf16[512,512]{1,0:T(8,128)(2,1)S(1)}, bf16[512,512]{1,0:T(8,128)(2,1)}, u32[]{:S(2)}) copy-start(bf16[512,512]{1,0:T(8,128)(2,1)} %param.22) | copy-start | bytes 1572868
  7.4 18.0 %all-gather.8.cloned.1.call-start = ((), (), s32[]{:S(2)}) async-start(), calls=%async_computation.7 | async-start | bytes 2359296 | tf_op jit(solution)/shard_map/all_gather | solution.py:113
  30.2 92.7 %all-to-all-start = ((bf16[4,1,384,2048]{3,2,1,0:T(8,128)(2,1)}), bf16[4,1,384,2048]{3,2,1,0:T(8,128)(2,1)}, u32[]{:S(2)}, u32[]{:S(2)}) async-start(bf16[4,1,384,2048]{3,2,1,0:T(8,128)(2,1)} %stack.3), calls=%async_computation | async-start | bytes 12582912 | tf_op jit(solution)/shard_map/all_to_all | solution.py:129
  35.5 50.7 %copy-start.6 = (f32[512]{0:T(512)S(1)}, f32[512]{0:T(512)}, u32[]{:S(2)}) copy-start(f32[512]{0:T(512)} %param.25) | copy-start | bytes 6148
  35.5 230.0 %all-gather.10.cloned.1.call-start = ((), (), s32[]{:S(2)}) async-start(), calls=%async_computation.8 | async-start | bytes 2621440 | tf_op jit(solution)/shard_map/all_gather | solution.py:183
  128.3 14.2 %all-to-all-start.3 = ((bf16[4,384,128]{2,1,0:T(8,128)(2,1)}), bf16[4,384,128]{2,1,0:T(8,128)(2,1)S(1)}, u32[]{:S(2)}, u32[]{:S(2)}) async-start(bf16[4,384,128]{2,1,0:T(8,128)(2,1)} %bitcast.16), calls=%async_computation.3 | async-start | bytes 786432 | tf_op jit(solution)/shard_map/all_to_all | solution.py:143
  137.1 9.5 %copy-start.5 = (f32[1,384,4]{1,2,0:T(4,128)S(1)}, f32[1,384,4]{1,2,0:T(4,128)}, u32[]{:S(2)}) copy-start(f32[1,384,4]{1,2,0:T(4,128)} %param.26) | copy-start | bytes 18436
  142.5 10.0 %all-to-all-start.4 = ((bf16[4,384,128]{2,1,0:T(8,128)(2,1)}), bf16[4,384,128]{2,1,0:T(8,128)(2,1)S(1)}, u32[]{:S(2)}, u32[]{:S(2)}) async-start(bf16[4,384,128]{2,1,0:T(8,128)(2,1)} %bitcast.31), calls=%async_computation.4 | async-start | bytes 786432 | tf_op jit(solution)/shard_map/all_to_all | solution.py:143
  147.5 1.0 copy-start.2
  152.6 9.3 %all-to-all-start.5 = ((bf16[4,384,128]{2,1,0:T(8,128)(2,1)}), bf16[4,384,128]{2,1,0:T(8,128)(2,1)S(1)}, u32[]{:S(2)}, u32[]{:S(2)}) async-start(bf16[4,384,128]{2,1,0:T(8,128)(2,1)} %bitcast.34), calls=%async_computation.5 | async-start | bytes 786432 | tf_op jit(solution)/shard_map/all_to_all | solution.py:143
  156.0 113.8 %all-gather.14.cloned.1.call-start = ((), (), s32[]{:S(2)}) async-start(), calls=%async_computation.11 | async-start | bytes 1310720 | tf_op jit(solution)/shard_map/all_gather | solution.py:26
  184.7 0.7 copy-start.1
  233.3 9.3 %all-to-all-start.2 = ((bf16[4,384,128]{1,2,0:T(8,128)(2,1)}), bf16[4,384,128]{1,2,0:T(8,128)(2,1)S(1)}, u32[]{:S(2)}, u32[]{:S(2)}) async-start(bf16[4,384,128]{1,2,0:T(8,128)(2,1)} %copy.28), calls=%async_computation.2 | async-start | bytes 786432 | tf_op jit(solution)/shard_map/all_to_all | solution.py:143
  236.8 10.4 %copy-start.8 = (f32[3,512]{1,0:T(4,128)S(1)}, f32[3,512]{1,0:T(4,128)}, u32[]{:S(2)}) copy-start(f32[3,512]{1,0:T(4,128)} %param.24) | copy-start | bytes 18436
  236.8 10.4 %copy-start.4 = (f32[6,4,64,128]{3,2,0,1:T(8,128)S(1)}, f32[6,4,64,128]{3,2,0,1:T(8,128)}, u32[]{:S(2)}) copy-start(f32[6,4,64,128]{3,2,0,1:T(8,128)} %get-tuple-element.142) | copy-start | bytes 2359300
  241.5 11.1 %copy-start.7 = (f32[4,128]{1,0:T(4,128)S(1)}, f32[4,128]{1,0:T(4,128)}, u32[]{:S(2)}) copy-start(f32[4,128]{1,0:T(4,128)} %get-tuple-element.227) | copy-start | bytes 6148
  242.6 9.8 %all-to-all-start.1 = ((bf16[4,384,128]{1,2,0:T(8,128)(2,1)}), bf16[4,384,128]{1,2,0:T(8,128)(2,1)S(1)}, u32[]{:S(2)}, u32[]{:S(2)}) async-start(bf16[4,384,128]{1,2,0:T(8,128)(2,1)} %copy.27), calls=%async_computation.1 | async-start | bytes 786432 | tf_op jit(solution)/shard_map/all_to_all | solution.py:143
  246.6 36.8 %all-gather.12.cloned.1.call-start = ((), (), s32[]{:S(2)}) async-start(), calls=%async_computation.9 | async-start | bytes 2621440 | tf_op jit(solution)/shard_map/all_gather | solution.py:184
  247.1 52.7 %reduce-scatter.2.cloned.1.call-start = ((), (), s32[]{:S(2)}) async-start(), calls=%async_computation.10 | async-start | bytes 4718592 | tf_op jit(solution)/shard_map/reduce_scatter | solution.py:186
  247.6 16.8 %collective-permute-start = (bf16[2,512]{0,1:T(8,128)(2,1)S(1)}, bf16[2,512]{0,1:T(8,128)(2,1)S(1)}, u32[]{:S(2)}, u32[]{:S(2)}) collective-permute-start(bf16[2,512]{0,1:T(8,128)(2,1)S(1)} %bitcast.196), channel_id=1, source_target_pairs={{0,8},{8,16},{16,24},{1,9},{9,17},{17,25},{2,10},{10,18},{18,26},{... | collective-permute-start | bytes 6152 | tf_op jit(solution)/shard_map/ppermute | solution.py:21
  269.8 3.7 %copy-start.3 = (f32[4,384,128]{2,1,0:T(8,128)S(1)}, f32[4,384,128]{2,1,0:T(8,128)}, u32[]{:S(2)}) copy-start(f32[4,384,128]{2,1,0:T(8,128)} %get-tuple-element.229) | copy-start | bytes 2359300
  269.8 4.8 %copy-start.9 = (f32[128]{0:T(128)S(1)}, f32[128]{0:T(128)}, u32[]{:S(2)}) copy-start(f32[128]{0:T(128)} %param.27) | copy-start | bytes 1540
Sparse Core Ops, SparseCore 0:
  12.9 12.5 all-gather.7
  288.7 11.1 reduce-scatter.1
Sparse Core Ops, SparseCore 1:
  37.8 76.3 all-gather.9
  185.6 39.6 all-gather.13
  248.9 34.4 all-gather.11
